TPU v7x, 32 devices: a whole 2x2x4 slice. The times are simulated.
32 devices in a mesh: sp: 8 (over z, y), tp: 4 (over x, core).
Axes of the slice: x: 2, y: 2, z: 4, core: 2. Of those that a mesh axis runs over, the one named last changes fastest.
Arguments:
- queries: bfloat16 [4096, 1024], P('sp', 'tp'), may hold values from -6 to 6
- key_heads: bfloat16 [4096, 512], P('sp', 'tp'), may hold values from -6 to 6
- value_heads: bfloat16 [4096, 512], P('sp', 'tp'), may hold values from -70 to 70
- documents: int32 [4096], P('sp'), may hold values from 0 to 2, never falling along the last dimension, each value on 1 to 2560 neighbouring positions
- query_gain: float32 [128], replicated, may hold values from 0.1 to 8
- key_gain: float32 [128], replicated, may hold values from 0.1 to 8
- out_gain: float32 [1024], replicated, may hold values from 0.1 to 1.9
- out_proj: bfloat16 [1024, 2048], replicated, may hold values from -0.1875 to 0.1875
- residual: bfloat16 [4096, 2048], P(('sp', 'tp')), may hold values from -6 to 6
- mid_gain: float32 [2048], replicated, may hold values from 0.1 to 1.9
- mid_bias: float32 [2048], replicated, may hold values from -1.5 to 1.5
- routes: int32 [4096, 2], P(('sp', 'tp')), may hold values from 0 to 31, all different within a row; in each aligned block of 128 rows (0 to 127, 128 to 255, ...) at most 16 rows name the same one
- route_weights: float32 [4096, 2], P(('sp', 'tp')), may hold values from 0.2 to 2
- expert_gate: bfloat16 [32, 2048, 512], P(('sp', 'tp')), may hold values from -0.125 to 0.125
- expert_up: bfloat16 [32, 2048, 512], P(('sp', 'tp')), may hold values from -0.125 to 0.125
- expert_down: bfloat16 [32, 512, 2048], P(('sp', 'tp')), may hold values from -0.25 to 0.25
- final_gain: float32 [2048], replicated, may hold values from 0.1 to 1.9
- final_bias: float32 [2048], replicated, may hold values from -1.5 to 1.5
Outputs:
- layer_out: bfloat16 [4096, 2048], P(('sp', 'tp'))
Inputs may be any that keep to these rules, and one draw needn't show every extreme that they name: `documents`: never falls along the sequence; each document holds 1 to 2560 positions and one holds exactly 2560. `routes`: each row names 2 different experts; among the rows of one device (aligned blocks of 128 rows) no expert is named more than 16 times, and exactly 16 times in some block.
All inputs are finite; a program needn't handle non-finite values.
Results may differ from a plain program's by a relative error of at most 0.014.
The roundings to bfloat16 on the way count: a program that leaves them out, or rounds other values in their place, can miss the bound.
Values may be sent and summed in bfloat16 or wider, within the bound.
A program may use at most 128 MiB of HBM per device.

v0:
```python
import math

import jax
import jax.numpy as jnp
from jax import lax
from jax.sharding import PartitionSpec as P

HEAD = 128
GRID = 64


eps_norm = 1e-06
alpha_mix = 8.0**0.25
theta_base = 10000.0


def rotary_tables(row_total, offset):
    positions = offset + jnp.arange(row_total, dtype=jnp.int32)
    grid_row = (positions // GRID).astype(jnp.float32)
    grid_col = (positions % GRID).astype(jnp.float32)
    pair_count = HEAD // 4
    inv_freq = theta_base ** (-jnp.arange(pair_count, dtype=jnp.float32) / pair_count)
    angles = jnp.concatenate(
        [grid_row[:, None] * inv_freq[None, :], grid_col[:, None] * inv_freq[None, :]], axis=1
    )
    return (jnp.cos(angles), jnp.sin(angles))


def normed_rotated(heads_in, gain_vec, cosine_table, sine_table):
    values = heads_in.astype(jnp.float32)
    inv_rms = lax.rsqrt(jnp.mean(values * values, axis=-1, keepdims=True) + eps_norm)
    values = values * inv_rms * gain_vec
    half_dim = HEAD // 2
    first_half = values[..., :half_dim]
    second_half = values[..., half_dim:]
    cosine_part = cosine_table[:, None, :]
    sine_part = sine_table[:, None, :]
    turned = jnp.concatenate(
        [
            first_half * cosine_part - second_half * sine_part,
            second_half * cosine_part + first_half * sine_part,
        ],
        axis=-1,
    )
    return turned.astype(jnp.bfloat16)


def layer_norm(stream, gain_vec, bias_vec):
    center = jnp.mean(stream, axis=-1, keepdims=True)
    spread = jnp.mean(jnp.square(stream - center), axis=-1, keepdims=True)
    return (stream - center) * lax.rsqrt(spread + eps_norm) * gain_vec + bias_vec


def per_device(
    queries,
    key_heads,
    value_heads,
    documents,
    query_gain,
    key_gain,
    out_gain,
    out_proj,
    residual,
    mid_gain,
    mid_bias,
    routes,
    route_weights,
    expert_gate,
    expert_up,
    expert_down,
    final_gain,
    final_bias,
):
    tok_rows = queries.shape[0]
    query_local = queries.shape[1] // HEAD
    key_local = key_heads.shape[1] // HEAD
    grouped = query_local // key_local
    offset = lax.axis_index("sp") * tok_rows
    cosine_table, sine_table = rotary_tables(tok_rows, offset)
    query_rot = normed_rotated(
        queries.reshape(tok_rows, query_local, HEAD), query_gain, cosine_table, sine_table
    ).reshape(tok_rows, key_local, grouped, HEAD)
    key_rot = normed_rotated(
        key_heads.reshape(tok_rows, key_local, HEAD), key_gain, cosine_table, sine_table
    ).reshape(tok_rows, key_local * HEAD)
    first_doc = documents[0]
    last_doc = documents[tok_rows - 1]
    start_state = (
        jnp.full((key_local, grouped, tok_rows), -1e30, jnp.float32),
        jnp.zeros((key_local, grouped, tok_rows), jnp.float32),
        jnp.zeros((key_local, grouped, tok_rows, HEAD), jnp.float32),
    )
    key_part = lax.all_gather(key_rot, "sp", axis=0, tiled=True)
    value_part = lax.all_gather(value_heads, "sp", axis=0, tiled=True)
    doc_part = lax.all_gather(documents, "sp", axis=0, tiled=True)
    piece_rows = key_part.shape[0]
    block_rows = math.gcd(piece_rows, 512)
    block_count = piece_rows // block_rows
    blocks = (
        key_part.reshape(block_count, block_rows, key_local, HEAD),
        value_part.reshape(block_count, block_rows, key_local, HEAD),
        doc_part.reshape(block_count, block_rows),
    )

    def advance(running, block_set):
        key_block, value_block, doc_block = block_set
        running_max, running_total, running_sum = running
        scores = jnp.einsum(
            "qkgd,tkd->kgqt", query_rot, key_block, preferred_element_type=jnp.float32
        ) * HEAD ** (-0.5)
        allowed = (documents[:, None] == doc_block[None, :])[None, None]
        scores = jnp.where(allowed, scores, -1e30)
        new_max = jnp.maximum(running_max, jnp.max(scores, axis=-1))
        weights = jnp.where(allowed, jnp.exp(scores - new_max[..., None]), 0.0)
        rescale = jnp.exp(running_max - new_max)
        new_total = running_total * rescale + jnp.sum(weights, axis=-1)
        new_sum = running_sum * rescale[..., None] + jnp.einsum(
            "kgqt,tkd->kgqd",
            weights.astype(jnp.bfloat16),
            value_block,
            preferred_element_type=jnp.float32,
        )
        return ((new_max, new_total, new_sum), None)

    def process(running):
        result, unused = lax.scan(advance, running, blocks)
        return result

    touches = (doc_part[0] <= last_doc) & (doc_part[piece_rows - 1] >= first_doc)
    final_max, final_total, final_sum = lax.cond(
        touches, process, lambda running: running, start_state
    )
    attention = jnp.transpose(final_sum / final_total[..., None], (2, 0, 1, 3))
    attention = attention.reshape(tok_rows, query_local * HEAD).astype(jnp.bfloat16)
    whole_rows = lax.all_to_all(attention, "tp", split_axis=0, concat_axis=1, tiled=True)
    whole_float = whole_rows.astype(jnp.float32)
    mean_square = jnp.mean(whole_float * whole_float, axis=1)
    scaled = (whole_float * out_gain).astype(jnp.bfloat16)
    projected = jnp.dot(scaled, out_proj, preferred_element_type=jnp.float32)
    projected = projected * lax.rsqrt(mean_square + eps_norm)[:, None]
    middle = layer_norm(
        alpha_mix * residual.astype(jnp.float32) + projected, mid_gain, mid_bias
    ).astype(jnp.bfloat16)
    out_rows = middle.shape[0]
    model_width = middle.shape[1]
    top_count = routes.shape[1]
    local_experts = expert_gate.shape[0]
    sp_size = lax.axis_size("sp")
    tp_size = lax.axis_size("tp")
    expert_total = local_experts * sp_size * tp_size
    capacity = 2 * out_rows * top_count // expert_total
    flat_routes = routes.reshape(-1)
    one_hot = (flat_routes[:, None] == jnp.arange(expert_total, dtype=jnp.int32)[None, :]).astype(
        jnp.int32
    )
    rank_in = jnp.sum((jnp.cumsum(one_hot, axis=0) - one_hot) * one_hot, axis=1)
    target = flat_routes * capacity + rank_in
    outbound = (
        jnp.zeros((expert_total * capacity, model_width), jnp.bfloat16)
        .at[target]
        .set(jnp.repeat(middle, top_count, axis=0))
    )
    arrived = lax.all_to_all(
        outbound.reshape(expert_total, capacity, model_width),
        ("sp", "tp"),
        split_axis=0,
        concat_axis=0,
        tiled=True,
    )
    item_count = arrived.shape[-2]
    grouped_rows = arrived.reshape(-1, local_experts, item_count, model_width)
    gate_part = jnp.einsum(
        "sekd,edf->sekf", grouped_rows, expert_gate, preferred_element_type=jnp.float32
    )
    up_part = jnp.einsum(
        "sekd,edf->sekf", grouped_rows, expert_up, preferred_element_type=jnp.float32
    )
    hidden = (jax.nn.silu(gate_part) * up_part).astype(jnp.bfloat16)
    served = jnp.einsum("sekf,efd->sekd", hidden, expert_down, preferred_element_type=jnp.float32)
    returned = lax.all_to_all(
        served.astype(jnp.bfloat16).reshape(arrived.shape),
        ("sp", "tp"),
        split_axis=0,
        concat_axis=0,
        tiled=True,
    )
    picked = returned.reshape(expert_total * capacity, model_width)[target]
    picked = picked.astype(jnp.float32).reshape(out_rows, top_count, model_width)
    routed = jnp.sum(picked * route_weights[:, :, None], axis=1)
    return layer_norm(
        alpha_mix * middle.astype(jnp.float32) + routed, final_gain, final_bias
    ).astype(jnp.bfloat16)


def solution(mesh):
    return jax.shard_map(
        per_device,
        mesh=mesh,
        in_specs=(
            P("sp", "tp"),
            P("sp", "tp"),
            P("sp", "tp"),
            P("sp"),
            P(),
            P(),
            P(),
            P(),
            P(("sp", "tp"), None),
            P(),
            P(),
            P(("sp", "tp"), None),
            P(("sp", "tp"), None),
            P(("sp", "tp"), None, None),
            P(("sp", "tp"), None, None),
            P(("sp", "tp"), None, None),
            P(),
            P(),
        ),
        out_specs=P(("sp", "tp"), None),
        check_vma=False,
    )
```

profile of v0, /device:TPU:13, one launch (start us, length us, event | category | flops | bytes accessed | tf_op | source)
XLA Modules:
  0.0 319.3 jit_solution(3362261494470061725)
XLA Ops:
  6.6 1.2 copy.46
  11.2 21.1 %all-gather = s32[8,1,512]{2,1,0:T(1,128)S(1)} all-gather(s32[1,1,512]{2,1,0:T(1,128)S(1)} %bitcast.186), channel_id=1, replica_groups=mesh['sp'=8,'tp'=4] {'sp'}, dimensions={0}, use_global_device_ids=true | all-gather | bytes 18432 | tf_op jit(solution)/shard_map/all_gather | solution.py:95
  38.0 10.4 %all-gather.4.cloned.1.call-done = bf16[4096,128]{0,1:T(8,128)(2,1)} async-done(((bf16[512,128]{0,1:T(8,128)(2,1)}), bf16[4096,128]{0,1:T(8,128)(2,1)}) %all-gather.4.cloned.1.call-update) | async-done | bytes 1048592 | tf_op jit(solution)/shard_map/all_gather | solution.py:93
  48.4 40.8 %all-gather.6.cloned.1.call-done = bf16[4096,128]{1,0:T(8,128)(2,1)} async-done(((bf16[512,128]{1,0:T(8,128)(2,1)}), bf16[4096,128]{1,0:T(8,128)(2,1)}) %all-gather.6.cloned.1.call-update) | async-done | bytes 1048592 | tf_op jit(solution)/shard_map/all_gather | solution.py:94
  89.2 69.2 %conditional.1 = (f32[1,2,512]{2,1,0:T(2,128)}, f32[1,2,512,128]{3,2,1,0:T(8,128)}) conditional(s32[]{:T(128)} %bitcast.4, () %tuple.17, (bf16[4096,128]{0,1:T(8,128)(2,1)}, bf16[4096,128]{1,0:T(8,128)(2,1)}, s32[4096]{0:T(1024)S(1)}, s32[512]{0:T(512)S(1)}, bf16[512,1,2,128]{0,3,2,1:T(8,128)(2,1)S(1)}) %tuple.62), branch_computations={%region_2.3_spmd, %region_3.8_spmd} | conditional | flops 275912704 | bytes 20030728 | solution.py:130
  89.2 2.3 copy.48
  91.7 66.7 %while.14 = (s32[]{:T(128)}, f32[1,2,512]{2,1,0:T(2,128)S(1)}, f32[1,2,512]{2,1,0:T(2,128)}, f32[1,2,512,128]{3,2,1,0:T(8,128)}, s32[512]{0:T(512)S(1)}, /*index...) while((s32[]{:T(128)}, f32[1,2,512]{2,1,0:T(2,128)S(1)}, ...), condition=%wide.region_7.7_spmd.clone, body=%wide.region_4.6_spmd.clone.sunk | while | flops 275912704 | bytes 17376408 | solution.py:126
  92.0 2.8 fusion.93
  94.8 3.4 %fusion.96 = f32[1,2,512,128]{3,2,1,0:T(8,128)} fusion(f32[512,512,2]{1,0,2:T(8,128)} %get-tuple-element.223, f32[2,512]{1,0:T(2,128)S(1)} %bitcast.183, pred[512,512]{0,1:T(8,128)(4,1)S(1)} %broadcast_compare_fusion.2, f32[1,2,512,128]{3,2,1,0:T(8,128)} %get-tuple-element.239, f32[2,512]{1,0:T(2,128)S(1)} %get-tuple-element.224, pred[]{:T(512)S(6)} %compare.14, ...), kind=kOutput, calls=%fused_computation.8.clone.1 | convolution fusion | flops 137232384 | bytes 3547649 | tf_op jit(solution)/shard_map/cond/branch_1_fun/while/body/eval_jaxpr/kgqt,tkd->kgqd/dot_general | solution.py:117
  99.6 2.8 fusion.93
  102.4 3.5 %fusion.96 = f32[1,2,512,128]{3,2,1,0:T(8,128)} fusion(f32[512,512,2]{1,0,2:T(8,128)} %get-tuple-element.223, f32[2,512]{1,0:T(2,128)S(1)} %bitcast.183, pred[512,512]{0,1:T(8,128)(4,1)S(1)} %broadcast_compare_fusion.2, f32[1,2,512,128]{3,2,1,0:T(8,128)} %get-tuple-element.239, f32[2,512]{1,0:T(2,128)S(1)} %get-tuple-element.224, pred[]{:T(512)S(6)} %compare.14, ...), kind=kOutput, calls=%fused_computation.8.clone.1 | convolution fusion | flops 137232384 | bytes 3547649 | tf_op jit(solution)/shard_map/cond/branch_1_fun/while/body/eval_jaxpr/kgqt,tkd->kgqd/dot_general | solution.py:117
  106.5 1.3 bitcast_add_fusion.2
  108.0 2.8 fusion.93
  110.9 3.5 %fusion.96 = f32[1,2,512,128]{3,2,1,0:T(8,128)} fusion(f32[512,512,2]{1,0,2:T(8,128)} %get-tuple-element.223, f32[2,512]{1,0:T(2,128)S(1)} %bitcast.183, pred[512,512]{0,1:T(8,128)(4,1)S(1)} %broadcast_compare_fusion.2, f32[1,2,512,128]{3,2,1,0:T(8,128)} %get-tuple-element.239, f32[2,512]{1,0:T(2,128)S(1)} %get-tuple-element.224, pred[]{:T(512)S(6)} %compare.14, ...), kind=kOutput, calls=%fused_computation.8.clone.1 | convolution fusion | flops 137232384 | bytes 3547649 | tf_op jit(solution)/shard_map/cond/branch_1_fun/while/body/eval_jaxpr/kgqt,tkd->kgqd/dot_general | solution.py:117
  115.0 1.3 bitcast_add_fusion.2
  116.5 2.8 fusion.93
  119.3 3.5 %fusion.96 = f32[1,2,512,128]{3,2,1,0:T(8,128)} fusion(f32[512,512,2]{1,0,2:T(8,128)} %get-tuple-element.223, f32[2,512]{1,0:T(2,128)S(1)} %bitcast.183, pred[512,512]{0,1:T(8,128)(4,1)S(1)} %broadcast_compare_fusion.2, f32[1,2,512,128]{3,2,1,0:T(8,128)} %get-tuple-element.239, f32[2,512]{1,0:T(2,128)S(1)} %get-tuple-element.224, pred[]{:T(512)S(6)} %compare.14, ...), kind=kOutput, calls=%fused_computation.8.clone.1 | convolution fusion | flops 137232384 | bytes 3547649 | tf_op jit(solution)/shard_map/cond/branch_1_fun/while/body/eval_jaxpr/kgqt,tkd->kgqd/dot_general | solution.py:117
  123.4 1.3 bitcast_add_fusion.2
  124.9 2.8 fusion.93
  127.7 3.5 %fusion.96 = f32[1,2,512,128]{3,2,1,0:T(8,128)} fusion(f32[512,512,2]{1,0,2:T(8,128)} %get-tuple-element.223, f32[2,512]{1,0:T(2,128)S(1)} %bitcast.183, pred[512,512]{0,1:T(8,128)(4,1)S(1)} %broadcast_compare_fusion.2, f32[1,2,512,128]{3,2,1,0:T(8,128)} %get-tuple-element.239, f32[2,512]{1,0:T(2,128)S(1)} %get-tuple-element.224, pred[]{:T(512)S(6)} %compare.14, ...), kind=kOutput, calls=%fused_computation.8.clone.1 | convolution fusion | flops 137232384 | bytes 3547649 | tf_op jit(solution)/shard_map/cond/branch_1_fun/while/body/eval_jaxpr/kgqt,tkd->kgqd/dot_general | solution.py:117
  131.8 1.3 bitcast_add_fusion.2
  133.3 2.8 fusion.93
  136.2 3.5 %fusion.96 = f32[1,2,512,128]{3,2,1,0:T(8,128)} fusion(f32[512,512,2]{1,0,2:T(8,128)} %get-tuple-element.223, f32[2,512]{1,0:T(2,128)S(1)} %bitcast.183, pred[512,512]{0,1:T(8,128)(4,1)S(1)} %broadcast_compare_fusion.2, f32[1,2,512,128]{3,2,1,0:T(8,128)} %get-tuple-element.239, f32[2,512]{1,0:T(2,128)S(1)} %get-tuple-element.224, pred[]{:T(512)S(6)} %compare.14, ...), kind=kOutput, calls=%fused_computation.8.clone.1 | convolution fusion | flops 137232384 | bytes 3547649 | tf_op jit(solution)/shard_map/cond/branch_1_fun/while/body/eval_jaxpr/kgqt,tkd->kgqd/dot_general | solution.py:117
  140.3 1.3 bitcast_add_fusion.2
  141.8 2.8 fusion.93
  144.6 3.5 %fusion.96 = f32[1,2,512,128]{3,2,1,0:T(8,128)} fusion(f32[512,512,2]{1,0,2:T(8,128)} %get-tuple-element.223, f32[2,512]{1,0:T(2,128)S(1)} %bitcast.183, pred[512,512]{0,1:T(8,128)(4,1)S(1)} %broadcast_compare_fusion.2, f32[1,2,512,128]{3,2,1,0:T(8,128)} %get-tuple-element.239, f32[2,512]{1,0:T(2,128)S(1)} %get-tuple-element.224, pred[]{:T(512)S(6)} %compare.14, ...), kind=kOutput, calls=%fused_computation.8.clone.1 | convolution fusion | flops 137232384 | bytes 3547649 | tf_op jit(solution)/shard_map/cond/branch_1_fun/while/body/eval_jaxpr/kgqt,tkd->kgqd/dot_general | solution.py:117
  148.7 1.3 bitcast_add_fusion.2
  150.2 2.8 fusion.93
  153.0 3.5 %fusion.96 = f32[1,2,512,128]{3,2,1,0:T(8,128)} fusion(f32[512,512,2]{1,0,2:T(8,128)} %get-tuple-element.223, f32[2,512]{1,0:T(2,128)S(1)} %bitcast.183, pred[512,512]{0,1:T(8,128)(4,1)S(1)} %broadcast_compare_fusion.2, f32[1,2,512,128]{3,2,1,0:T(8,128)} %get-tuple-element.239, f32[2,512]{1,0:T(2,128)S(1)} %get-tuple-element.224, pred[]{:T(512)S(6)} %compare.14, ...), kind=kOutput, calls=%fused_computation.8.clone.1 | convolution fusion | flops 137232384 | bytes 3547649 | tf_op jit(solution)/shard_map/cond/branch_1_fun/while/body/eval_jaxpr/kgqt,tkd->kgqd/dot_general | solution.py:117
  157.1 1.3 bitcast_add_fusion.2
  158.4 1.3 fusion.57
  159.9 0.9 convert_element_type.116
  160.8 4.9 %all-to-all-start = ((bf16[4,128,256]{2,1,0:T(8,128)(2,1)}), bf16[4,128,256]{2,1,0:T(8,128)(2,1)S(1)}, u32[]{:S(2)}, u32[]{:S(2)}) async-start(bf16[4,128,256]{2,1,0:T(8,128)(2,1)} %convert_element_type.116), calls=%async_computation | async-start | bytes 524288 | tf_op jit(solution)/shard_map/all_to_all | solution.py:135
  165.7 5.0 %all-to-all-done = bf16[4,128,256]{2,1,0:T(8,128)(2,1)S(1)} async-done(((bf16[4,128,256]{2,1,0:T(8,128)(2,1)}), bf16[4,128,256]{2,1,0:T(8,128)(2,1)S(1)}, u32[]{:S(2)}, u32[]{:S(2)}) %all-to-all-start) | async-done | bytes 262176 | tf_op jit(solution)/shard_map/all_to_all | solution.py:135
  171.4 3.1 fusion.80
  175.1 1.6 broadcast_in_dim.43
  176.7 2.3 reshape.481
  178.9 4.4 %scatter_custom_fusion = bf16[512,2048]{1,0:T(8,128)(2,1)} fusion(s32[256]{0:T(256)S(1)} %bitcast.190, bf16[256,2048]{1,0:T(8,128)(2,1)} %reshape.481, bf16[]{:T(256)} %constant.103.clone.1), kind=kCustom, calls=%fused_computation.51 | custom fusion | bytes 2097664 | tf_op jit(solution)/shard_map/scatter | solution.py:161
  183.4 51.8 %all_to_all.20 = bf16[32,16,2048]{2,1,0:T(8,128)(2,1)S(1)} all-to-all(bf16[32,16,2048]{2,1,0:T(8,128)(2,1)} %bitcast.181), channel_id=1, replica_groups=mesh['sp'=8,'tp'=4] {'sp','tp'}, dimensions={0} | all-to-all | bytes 4194304 | tf_op jit(solution)/shard_map/all_to_all | solution.py:163
  235.2 1.3 copy-done.2
  236.5 2.2 fusion.29
  238.7 6.3 %convolution_convert_fusion = bf16[32,16,2048]{2,1,0:T(8,128)(2,1)} fusion(bf16[1,512,2048]{2,1,0:T(8,128)(2,1)S(1)} %copy-done, bf16[32,16,2048]{2,1,0:T(8,128)(2,1)} %copy-done.2, bf16[1,2048,512]{2,1,0:T(8,128)(2,1)} %param.36, f32[32,1,16,512]{3,2,0,1:T(8,128)} %fusion.29), kind=kOutput, calls=%fused_computation.35 | convolution fusion | flops 2150105088 | bytes 9437184 | tf_op jit(solution)/shard_map/sekf,efd->sekd/dot_general | solution.py:179
  245.0 6.2 %all-to-all-start.2 = ((bf16[32,16,2048]{2,1,0:T(8,128)(2,1)}), bf16[32,16,2048]{2,1,0:T(8,128)(2,1)}, u32[]{:S(2)}, u32[]{:S(2)}) async-start(bf16[32,16,2048]{2,1,0:T(8,128)(2,1)} %convolution_convert_fusion), calls=%async_computation.2 | async-start | bytes 4194304 | tf_op jit(solution)/shard_map/all_to_all | solution.py:180
  251.3 45.4 %all-to-all-done.2 = bf16[32,16,2048]{2,1,0:T(8,128)(2,1)} async-done(((bf16[32,16,2048]{2,1,0:T(8,128)(2,1)}), bf16[32,16,2048]{2,1,0:T(8,128)(2,1)}, u32[]{:S(2)}, u32[]{:S(2)}) %all-to-all-start.2) | async-done | bytes 2097184 | tf_op jit(solution)/shard_map/all_to_all | solution.py:180
  296.7 5.2 %gather_fusion = bf16[256,2048]{1,0:T(8,128)(2,1)} fusion(bf16[512,2048]{1,0:T(8,128)(2,1)} %bitcast.37, s32[1024]{0:T(1024)S(1)} %pad_clamp_fusion), kind=kCustom, calls=%fused_computation | custom fusion | bytes 2098176 | tf_op jit(solution)/shard_map/gather | solution.py:187
  301.9 3.4 %reshape.468 = f32[128,2,2048]{2,1,0:T(2,128)} reshape(bf16[256,2048]{1,0:T(8,128)(2,1)} %gather_fusion) | data formatting | bytes 3145728 | tf_op jit(solution)/shard_map/convert_element_type | solution.py:188
  305.3 4.8 %multiply_reduce_fusion = f32[128,2048]{1,0:T(8,128)S(1)} fusion(f32[128,2,2048]{2,1,0:T(2,128)} %reshape.468, f32[128,2]{1,0:T(8,128)S(1)} %copy.56), kind=kLoop, calls=%fused_computation.43 | loop fusion | flops 786432 | bytes 3146752 | tf_op jit(solution)/shard_map/reduce_sum | solution.py:189
  311.1 1.4 add_convert_fusion
  (137 shorter events, 16.3 us)
Async XLA Ops:
  6.5 232.1 %copy-start = (bf16[1,512,2048]{2,1,0:T(8,128)(2,1)S(1)}, bf16[1,512,2048]{2,1,0:T(8,128)(2,1)}, u32[]{:S(2)}) copy-start(bf16[1,512,2048]{2,1,0:T(8,128)(2,1)} %param.37) | copy-start | bytes 6291460
  6.5 4.1 %copy-start.10 = (s32[128,2]{0,1:T(2,128)S(1)}, s32[128,2]{0,1:T(2,128)}, u32[]{:S(2)}) copy-start(s32[128,2]{0,1:T(2,128)} %param.33) | copy-start | bytes 3076
  6.5 4.5 %copy-start.3 = (bf16[512,256]{1,0:T(8,128)(2,1)S(1)}, bf16[512,256]{1,0:T(8,128)(2,1)}, u32[]{:S(2)}) copy-start(bf16[512,256]{1,0:T(8,128)(2,1)} %param.22) | copy-start | bytes 786436
  6.5 4.7 %copy-start.6 = (s32[512]{0:T(512)S(1)}, s32[512]{0:T(512)}, u32[]{:S(2)}) copy-start(s32[512]{0:T(512)} %param.25) | copy-start | bytes 6148
  6.5 31.2 %copy-start.12 = (f32[128]{0:T(128)S(1)}, f32[128]{0:T(128)}, u32[]{:S(2)}) copy-start(f32[128]{0:T(128)} %param.26) | copy-start | bytes 1540
  6.5 41.8 %all-gather.4.cloned.1.call-start = ((), (), s32[]{:S(2)}) async-start(), calls=%async_computation.3 | async-start | bytes 1179648 | tf_op jit(solution)/shard_map/all_gather | solution.py:93
  9.9 79.3 %all-gather.6.cloned.1.call-start = ((), (), s32[]{:S(2)}) async-start(), calls=%async_computation.4 | async-start | bytes 1179648 | tf_op jit(solution)/shard_map/all_gather | solution.py:94
  94.8 3.4 %copy-start.1 = (f32[512,512,2]{1,0,2:T(8,128)S(1)}, f32[512,512,2]{1,0,2:T(8,128)}, u32[]{:S(2)}) copy-start(f32[512,512,2]{1,0,2:T(8,128)} %get-tuple-element.223) | copy-start | bytes 6291460 | tf_op jit(solution)/shard_map/cond/branch_1_fun/while
  102.4 3.5 %copy-start.1 = (f32[512,512,2]{1,0,2:T(8,128)S(1)}, f32[512,512,2]{1,0,2:T(8,128)}, u32[]{:S(2)}) copy-start(f32[512,512,2]{1,0,2:T(8,128)} %get-tuple-element.223) | copy-start | bytes 6291460 | tf_op jit(solution)/shard_map/cond/branch_1_fun/while
  110.9 3.5 %copy-start.1 = (f32[512,512,2]{1,0,2:T(8,128)S(1)}, f32[512,512,2]{1,0,2:T(8,128)}, u32[]{:S(2)}) copy-start(f32[512,512,2]{1,0,2:T(8,128)} %get-tuple-element.223) | copy-start | bytes 6291460 | tf_op jit(solution)/shard_map/cond/branch_1_fun/while
  119.3 3.5 %copy-start.1 = (f32[512,512,2]{1,0,2:T(8,128)S(1)}, f32[512,512,2]{1,0,2:T(8,128)}, u32[]{:S(2)}) copy-start(f32[512,512,2]{1,0,2:T(8,128)} %get-tuple-element.223) | copy-start | bytes 6291460 | tf_op jit(solution)/shard_map/cond/branch_1_fun/while
  127.7 3.5 %copy-start.1 = (f32[512,512,2]{1,0,2:T(8,128)S(1)}, f32[512,512,2]{1,0,2:T(8,128)}, u32[]{:S(2)}) copy-start(f32[512,512,2]{1,0,2:T(8,128)} %get-tuple-element.223) | copy-start | bytes 6291460 | tf_op jit(solution)/shard_map/cond/branch_1_fun/while
  136.2 3.5 %copy-start.1 = (f32[512,512,2]{1,0,2:T(8,128)S(1)}, f32[512,512,2]{1,0,2:T(8,128)}, u32[]{:S(2)}) copy-start(f32[512,512,2]{1,0,2:T(8,128)} %get-tuple-element.223) | copy-start | bytes 6291460 | tf_op jit(solution)/shard_map/cond/branch_1_fun/while
  144.6 3.5 %copy-start.1 = (f32[512,512,2]{1,0,2:T(8,128)S(1)}, f32[512,512,2]{1,0,2:T(8,128)}, u32[]{:S(2)}) copy-start(f32[512,512,2]{1,0,2:T(8,128)} %get-tuple-element.223) | copy-start | bytes 6291460 | tf_op jit(solution)/shard_map/cond/branch_1_fun/while
  153.0 3.5 %copy-start.1 = (f32[512,512,2]{1,0,2:T(8,128)S(1)}, f32[512,512,2]{1,0,2:T(8,128)}, u32[]{:S(2)}) copy-start(f32[512,512,2]{1,0,2:T(8,128)} %get-tuple-element.223) | copy-start | bytes 6291460 | tf_op jit(solution)/shard_map/cond/branch_1_fun/while
  158.4 12.7 %copy-start.9 = (f32[1024]{0:T(1024)S(1)}, f32[1024]{0:T(1024)}, u32[]{:S(2)}) copy-start(f32[1024]{0:T(1024)} %param.28) | copy-start | bytes 12292
  160.8 9.9 %all-to-all-start = ((bf16[4,128,256]{2,1,0:T(8,128)(2,1)}), bf16[4,128,256]{2,1,0:T(8,128)(2,1)S(1)}, u32[]{:S(2)}, u32[]{:S(2)}) async-start(bf16[4,128,256]{2,1,0:T(8,128)(2,1)} %convert_element_type.116), calls=%async_computation | async-start | bytes 524288 | tf_op jit(solution)/shard_map/all_to_all | solution.py:135
  171.3 3.4 %copy-start.4 = (f32[2048]{0:T(1024)S(1)}, f32[2048]{0:T(1024)}, u32[]{:S(2)}) copy-start(f32[2048]{0:T(1024)} %param.32) | copy-start | bytes 24580
  171.3 3.4 %copy-start.5 = (f32[2048]{0:T(1024)S(1)}, f32[2048]{0:T(1024)}, u32[]{:S(2)}) copy-start(f32[2048]{0:T(1024)} %param.31) | copy-start | bytes 24580
  183.4 53.1 %copy-start.13 = (bf16[1,2048,512]{2,1,0:T(8,128)(2,1)S(1)}, bf16[1,2048,512]{2,1,0:T(8,128)(2,1)}, u32[]{:S(2)}) copy-start(bf16[1,2048,512]{2,1,0:T(8,128)(2,1)} %param.35) | copy-start | bytes 6291460
  235.2 1.3 copy-start.2
  244.9 6.2 %copy-start.11 = (f32[128,2]{0,1:T(2,128)S(1)}, f32[128,2]{0,1:T(2,128)}, u32[]{:S(2)}) copy-start(f32[128,2]{0,1:T(2,128)} %param.34) | copy-start | bytes 3076
  245.0 51.8 %all-to-all-start.2 = ((bf16[32,16,2048]{2,1,0:T(8,128)(2,1)}), bf16[32,16,2048]{2,1,0:T(8,128)(2,1)}, u32[]{:S(2)}, u32[]{:S(2)}) async-start(bf16[32,16,2048]{2,1,0:T(8,128)(2,1)} %convolution_convert_fusion), calls=%async_computation.2 | async-start | bytes 4194304 | tf_op jit(solution)/shard_map/all_to_all | solution.py:180
  310.1 0.9 copy-start.7
  310.1 0.9 copy-start.8
Sparse Core Ops, SparseCore 0:
  10.0 38.3 all-gather.3
  50.5 38.6 all-gather.5
where the time goes:
time: 325 us; the launch traced here: 319 us
  waiting for transfers between devices  102 us (31%)
  blocking collectives  72.8 us (22%)
  matrix products  62 us (19%)
  other arithmetic  28.8 us (9%)
  local copies, waits for them, and re-layouts  25.6 us (8%)
  between operations  16.2 us (5%)
  starting transfers between devices  11.2 us (3%)
    all_to_all x1, blocking collectives, per_device(): lax.all_to_all(outbound.reshape(expert_total, capacity, model_width), ('s...  51.8 us
    all_to_all x1, waiting for transfers between devices, per_device(): lax.all_to_all(served.astype(jnp.bfloat16).reshape(arrived.shape), ('sp',...  45.4 us
    all_gather x1, waiting for transfers between devices, per_device(): value_part = lax.all_gather(value_heads, 'sp', axis=0, tiled=True)  40.8 us
    dot_general x8, matrix products, advance(): jnp.einsum('kgqt,tkd->kgqd', weights.astype(jnp.bfloat16), value_block, p...  28 us
    dot_general x8, matrix products, advance(): jnp.einsum('qkgd,tkd->kgqt', query_rot, key_block, preferred_element_type...  22.4 us
    all_gather x1, blocking collectives, per_device(): doc_part = lax.all_gather(documents, 'sp', axis=0, tiled=True)  21.1 us
    all_gather x1, waiting for transfers between devices, per_device(): key_part = lax.all_gather(key_rot, 'sp', axis=0, tiled=True)  10.4 us
    add x8, other arithmetic, advance(): new_total = running_total * rescale + jnp.sum(weights, axis=-1)  9.54 us
  transfers between devices with their start and end apart: 4, of which 4 were waited for; matrix products, arithmetic and copies ran while one was open for 1% of the time, Pallas kernels for 0%

commit v1 on v0

v1 whole, which is shorter than its diff:
```python
import functools

import jax
import jax.numpy as jnp
from jax import lax
from jax.experimental import pallas as pl
from jax.experimental.pallas import tpu as pltpu
from jax.sharding import PartitionSpec as P

HEAD = 128
GRID = 64


eps_norm = 1e-06
alpha_mix = 8.0**0.25
theta_base = 10000.0
score_factor = HEAD ** (-0.5) * 1.4426950408889634
VMEM = pl.BlockSpec(memory_space=pltpu.VMEM)
ANY = pl.BlockSpec(memory_space=pl.ANY)
SMEM = pl.BlockSpec(memory_space=pltpu.SMEM)


def rotary_tables(row_total, offset):
    positions = offset + jnp.arange(row_total, dtype=jnp.int32)
    grid_row = (positions // GRID).astype(jnp.float32)
    grid_col = (positions % GRID).astype(jnp.float32)
    pair_count = HEAD // 4
    inv_freq = theta_base ** (-jnp.arange(pair_count, dtype=jnp.float32) / pair_count)
    angles = jnp.concatenate(
        [grid_row[:, None] * inv_freq[None, :], grid_col[:, None] * inv_freq[None, :]], axis=1
    )
    return (jnp.cos(angles), jnp.sin(angles))


def normed_rotated(heads_in, gain_vec, cosine_table, sine_table):
    values = heads_in.astype(jnp.float32)
    inv_rms = lax.rsqrt(jnp.mean(values * values, axis=-1, keepdims=True) + eps_norm)
    values = values * inv_rms * gain_vec
    half_dim = HEAD // 2
    first_half = values[..., :half_dim]
    second_half = values[..., half_dim:]
    cosine_part = cosine_table[:, None, :]
    sine_part = sine_table[:, None, :]
    turned = jnp.concatenate(
        [
            first_half * cosine_part - second_half * sine_part,
            second_half * cosine_part + first_half * sine_part,
        ],
        axis=-1,
    )
    return turned.astype(jnp.bfloat16)


def layer_norm(stream, gain_vec, bias_vec):
    center = jnp.mean(stream, axis=-1, keepdims=True)
    spread = jnp.mean(jnp.square(stream - center), axis=-1, keepdims=True)
    return (stream - center) * lax.rsqrt(spread + eps_norm) * gain_vec + bias_vec


def barrier_with(peers):
    barrier = pltpu.get_barrier_semaphore()
    for peer in peers:
        pl.semaphore_signal(barrier, inc=1, device_id=peer, device_id_type=pl.DeviceIdType.MESH)
    pl.semaphore_wait(barrier, len(peers))


def gather_kernel(
    size, pair, kv_ref, doc_ref, kv_all, doc_all, kv_send, kv_recv, doc_send, doc_recv, own_sem
):
    me = lax.axis_index("sp")
    inner = lax.rem(me, pair)
    outer = me // pair
    outer_size = size // pair
    own = [
        pltpu.make_async_copy(kv_ref, kv_all.at[me], own_sem.at[0]),
        pltpu.make_async_copy(doc_ref, doc_all.at[me], own_sem.at[1]),
    ]
    for copy in own:
        copy.start()
    far = [
        lax.rem(outer + step, outer_size) * pair + inner for step in range(1, outer_size)
    ]
    mate = outer * pair + lax.rem(inner + 1, pair)
    peers = [{"sp": index} for index in far]
    if pair == 2:
        peers.append({"sp": mate})
    barrier_with(peers)

    def send(from_kv, from_doc, place, slot, target):
        copies = (
            pltpu.make_async_remote_copy(
                src_ref=from_kv,
                dst_ref=kv_all.at[place],
                send_sem=kv_send.at[slot],
                recv_sem=kv_recv.at[slot],
                device_id={"sp": target},
                device_id_type=pl.DeviceIdType.MESH,
            ),
            pltpu.make_async_remote_copy(
                src_ref=from_doc,
                dst_ref=doc_all.at[place],
                send_sem=doc_send.at[slot],
                recv_sem=doc_recv.at[slot],
                device_id={"sp": target},
                device_id_type=pl.DeviceIdType.MESH,
            ),
        )
        for copy in copies:
            copy.start()
        return copies

    far_copies = []
    for step, target in enumerate(far):
        far_copies.append(send(kv_ref, doc_ref, me, step, target))
    mate_copies = []
    if pair == 2:
        mate_copies.append(send(kv_ref, doc_ref, me, outer_size - 1, mate))
    for step in range(1, outer_size):
        for copy in far_copies[step - 1]:
            copy.wait_recv()
        if pair == 2:
            place = lax.rem(outer - step + outer_size, outer_size) * pair + inner
            mate_copies.append(
                send(kv_all.at[place], doc_all.at[place], place, outer_size - 1 + step, mate)
            )
    for copies in mate_copies:
        for copy in copies:
            copy.wait_recv()
    for copies in far_copies + mate_copies:
        for copy in copies:
            copy.wait_send()
    for copy in own:
        copy.wait()


def gather_keys(kv, docs, size):
    pair = 2 if size % 2 == 0 else 1
    slots = max(size - 1, 1)
    return pl.pallas_call(
        functools.partial(gather_kernel, size, pair),
        out_shape=(
            jax.ShapeDtypeStruct((size,) + kv.shape, kv.dtype),
            jax.ShapeDtypeStruct((size,) + docs.shape, docs.dtype),
        ),
        in_specs=[ANY, ANY],
        out_specs=(ANY, ANY),
        scratch_shapes=[pltpu.SemaphoreType.DMA((slots,)) for unused in range(4)]
        + [pltpu.SemaphoreType.DMA((2,))],
        compiler_params=pltpu.CompilerParams(collective_id=0, has_side_effects=True),
    )(kv, docs)


def attention_kernel(grouped, q_ref, qdoc_ref, kv_ref, doc_ref, range_ref, o_ref, m_ref, l_ref, acc_ref):
    rows = q_ref.shape[1]
    block = kv_ref.shape[2]
    pieces = doc_ref.shape[1]
    chunk = 256
    m_ref[...] = jnp.full(m_ref.shape, -1e30, jnp.float32)
    l_ref[...] = jnp.zeros(l_ref.shape, jnp.float32)
    acc_ref[...] = jnp.zeros(acc_ref.shape, jnp.float32)

    def advance(number, unused):
        keys = kv_ref[number, 0]
        values = kv_ref[number, 1]
        doc_rows = doc_ref[number]
        key_docs = jnp.concatenate([doc_rows[i : i + 1] for i in range(pieces)], axis=1)
        for head in range(grouped):
            for first in range(0, rows, chunk):
                part = pl.ds(first, chunk)
                scores = lax.dot_general(
                    q_ref[head, part],
                    keys,
                    (((1,), (1,)), ((), ())),
                    preferred_element_type=jnp.float32,
                )
                allowed = qdoc_ref[part, 0:1] == key_docs
                scores = jnp.where(allowed, scores * score_factor, -1e30)
                old_max = m_ref[head, part]
                new_max = jnp.maximum(old_max, jnp.max(scores, axis=1, keepdims=True))
                base = jnp.maximum(new_max[:, 0:1], -1e29)
                weights = jnp.exp2(scores - base)
                rescale = jnp.exp2(old_max - new_max)
                l_ref[head, part] = l_ref[head, part] * rescale + jnp.sum(
                    weights, axis=1, keepdims=True
                )
                acc_ref[head, part] = acc_ref[head, part] * rescale + jnp.dot(
                    weights.astype(jnp.bfloat16), values, preferred_element_type=jnp.float32
                )
                m_ref[head, part] = new_max
        return unused

    lax.fori_loop(range_ref[0], range_ref[1], advance, 0)
    for head in range(grouped):
        o_ref[:, head * HEAD : (head + 1) * HEAD] = (acc_ref[head] / l_ref[head]).astype(
            o_ref.dtype
        )


def attend(query_rot, query_docs, kv_all, doc_all, block_range):
    grouped, rows, width = query_rot.shape
    return pl.pallas_call(
        functools.partial(attention_kernel, grouped),
        out_shape=jax.ShapeDtypeStruct((rows, grouped * width), jnp.bfloat16),
        in_specs=[VMEM, VMEM, VMEM, VMEM, SMEM],
        out_specs=VMEM,
        scratch_shapes=[pltpu.VMEM((grouped, rows, width), jnp.float32) for unused in range(3)],
        compiler_params=pltpu.CompilerParams(vmem_limit_bytes=48 * 1024 * 1024),
    )(query_rot, query_docs, kv_all, doc_all, block_range)


def head_exchange_kernel(size, x_ref, o_ref, send_sem, recv_sem, own_sem):
    me = lax.axis_index("tp")
    rows, width = o_ref.shape[0], x_ref.shape[1]
    mine = o_ref.at[:, pl.ds(pl.multiple_of(me * width, width), width)]
    own = pltpu.make_async_copy(
        x_ref.at[pl.ds(pl.multiple_of(me * rows, rows), rows)], mine, own_sem
    )
    own.start()
    targets = [lax.rem(me + step, size) for step in range(1, size)]
    barrier_with([{"tp": target} for target in targets])
    copies = []
    for step, target in enumerate(targets):
        copy = pltpu.make_async_remote_copy(
            src_ref=x_ref.at[pl.ds(pl.multiple_of(target * rows, rows), rows)],
            dst_ref=mine,
            send_sem=send_sem.at[step],
            recv_sem=recv_sem.at[step],
            device_id={"tp": target},
            device_id_type=pl.DeviceIdType.MESH,
        )
        copy.start()
        copies.append(copy)
    for copy in copies:
        copy.wait()
    own.wait()


def exchange_heads(attention, size):
    rows, width = attention.shape
    return pl.pallas_call(
        functools.partial(head_exchange_kernel, size),
        out_shape=jax.ShapeDtypeStruct((rows // size, width * size), attention.dtype),
        in_specs=[VMEM],
        out_specs=VMEM,
        scratch_shapes=[
            pltpu.SemaphoreType.DMA((size,)),
            pltpu.SemaphoreType.DMA((size,)),
            pltpu.SemaphoreType.DMA,
        ],
        compiler_params=pltpu.CompilerParams(collective_id=1, has_side_effects=True),
    )(attention)


def all_exchange_kernel(sp_size, tp_size, x_ref, o_ref, send_sem, recv_sem, own_sem):
    me = lax.axis_index("sp") * tp_size + lax.axis_index("tp")
    size = sp_size * tp_size
    own = pltpu.make_async_copy(x_ref.at[me], o_ref.at[me], own_sem)
    own.start()
    barrier = pltpu.get_barrier_semaphore()

    def greet(step, unused):
        target = lax.rem(me + step, size)
        pl.semaphore_signal(
            barrier,
            inc=1,
            device_id={"sp": target // tp_size, "tp": lax.rem(target, tp_size)},
            device_id_type=pl.DeviceIdType.MESH,
        )
        return unused

    lax.fori_loop(1, size, greet, 0)
    pl.semaphore_wait(barrier, size - 1)

    def copy_of(step):
        target = lax.rem(me + step, size)
        return pltpu.make_async_remote_copy(
            src_ref=x_ref.at[target],
            dst_ref=o_ref.at[me],
            send_sem=send_sem.at[step],
            recv_sem=recv_sem.at[step],
            device_id={"sp": target // tp_size, "tp": lax.rem(target, tp_size)},
            device_id_type=pl.DeviceIdType.MESH,
        )

    def begin(step, unused):
        copy_of(step).start()
        return unused

    def finish(step, unused):
        copy_of(step).wait()
        return unused

    lax.fori_loop(1, size, begin, 0)
    lax.fori_loop(1, size, finish, 0)
    own.wait()


def exchange_all(blocks, sp_size, tp_size, collective_id):
    size = blocks.shape[0]
    return pl.pallas_call(
        functools.partial(all_exchange_kernel, sp_size, tp_size),
        out_shape=jax.ShapeDtypeStruct(blocks.shape, blocks.dtype),
        in_specs=[ANY],
        out_specs=ANY,
        scratch_shapes=[
            pltpu.SemaphoreType.DMA((size,)),
            pltpu.SemaphoreType.DMA((size,)),
            pltpu.SemaphoreType.DMA,
        ],
        compiler_params=pltpu.CompilerParams(collective_id=collective_id, has_side_effects=True),
    )(blocks)


def middle_kernel(
    x_ref, gain_ref, proj_ref, res_ref, mid_gain_ref, mid_bias_ref, target_ref, mid_ref, out_ref
):
    whole = x_ref[...].astype(jnp.float32)
    mean_square = jnp.mean(whole * whole, axis=1, keepdims=True)
    scaled = (whole * gain_ref[...]).astype(jnp.bfloat16)
    projected = jnp.dot(scaled, proj_ref[...], preferred_element_type=jnp.float32)
    projected = projected * lax.rsqrt(mean_square + eps_norm)
    stream = alpha_mix * res_ref[...].astype(jnp.float32) + projected
    middle = layer_norm(stream, mid_gain_ref[...], mid_bias_ref[...]).astype(jnp.bfloat16)
    mid_ref[...] = middle
    slots, rows = out_ref.shape[0], middle.shape[0]
    slot = lax.broadcasted_iota(jnp.int32, (slots, rows), 0)
    chosen = slot == target_ref[0:1, :]
    for route in range(1, target_ref.shape[0]):
        chosen = chosen | (slot == target_ref[route : route + 1, :])
    select = jnp.where(chosen, 1.0, 0.0).astype(jnp.bfloat16)
    out_ref[...] = jnp.dot(select, middle, preferred_element_type=jnp.float32).astype(
        jnp.bfloat16
    )


def final_kernel(back_ref, target_ref, weight_ref, mid_ref, gain_ref, bias_ref, o_ref):
    rows, slots = mid_ref.shape[0], back_ref.shape[0]
    slot = lax.broadcasted_iota(jnp.int32, (rows, slots), 1)
    routed = None
    for route in range(target_ref.shape[1]):
        select = jnp.where(slot == target_ref[:, route : route + 1], 1.0, 0.0)
        picked = jnp.dot(
            select.astype(jnp.bfloat16), back_ref[...], preferred_element_type=jnp.float32
        )
        term = picked * weight_ref[:, route : route + 1]
        routed = term if routed is None else routed + term
    stream = alpha_mix * mid_ref[...].astype(jnp.float32) + routed
    o_ref[...] = layer_norm(stream, gain_ref[...], bias_ref[...]).astype(o_ref.dtype)


def per_device(
    queries,
    key_heads,
    value_heads,
    documents,
    query_gain,
    key_gain,
    out_gain,
    out_proj,
    residual,
    mid_gain,
    mid_bias,
    routes,
    route_weights,
    expert_gate,
    expert_up,
    expert_down,
    final_gain,
    final_bias,
):
    tok_rows = queries.shape[0]
    query_local = queries.shape[1] // HEAD
    key_local = key_heads.shape[1] // HEAD
    grouped = query_local // key_local
    sp_size = lax.axis_size("sp")
    tp_size = lax.axis_size("tp")
    offset = lax.axis_index("sp") * tok_rows
    cosine_table, sine_table = rotary_tables(tok_rows, offset)
    query_rot = normed_rotated(
        queries.reshape(tok_rows, query_local, HEAD), query_gain, cosine_table, sine_table
    )
    query_rot = jnp.transpose(query_rot, (1, 0, 2))
    key_rot = normed_rotated(
        key_heads.reshape(tok_rows, key_local, HEAD), key_gain, cosine_table, sine_table
    )
    values = value_heads.reshape(tok_rows, key_local, HEAD)
    query_docs = jnp.broadcast_to(documents[:, None], (tok_rows, HEAD))
    kv = jnp.transpose(jnp.stack([key_rot, values]), (2, 0, 1, 3))
    kv_all, doc_all = gather_keys(
        kv.reshape(key_local * 2, tok_rows, HEAD), documents.reshape(tok_rows // HEAD, HEAD), sp_size
    )
    low = jnp.sum((doc_all[:, -1, -1] < documents[0]).astype(jnp.int32))
    high = jnp.sum((doc_all[:, 0, 0] <= documents[tok_rows - 1]).astype(jnp.int32))
    block_range = jnp.stack([low, high])
    heads = []
    for head in range(key_local):
        heads.append(
            attend(
                query_rot[head * grouped : (head + 1) * grouped],
                query_docs,
                kv_all if key_local == 1 else kv_all[:, 2 * head : 2 * head + 2],
                doc_all,
                block_range,
            )
        )
    attention = heads[0] if key_local == 1 else jnp.concatenate(heads, axis=1)
    whole_rows = exchange_heads(attention, tp_size)
    out_rows, model_width = residual.shape
    top_count = routes.shape[1]
    local_experts = expert_gate.shape[0]
    device_total = sp_size * tp_size
    expert_total = local_experts * device_total
    capacity = 2 * out_rows * top_count // expert_total
    flat_routes = routes.T.reshape(-1)
    flat_total = flat_routes.shape[0]
    one_hot = flat_routes[:, None] == jnp.arange(expert_total, dtype=jnp.int32)[None, :]
    earlier = jnp.arange(flat_total)[:, None] > jnp.arange(flat_total)[None, :]
    before = jnp.dot(
        earlier.astype(jnp.bfloat16),
        one_hot.astype(jnp.bfloat16),
        preferred_element_type=jnp.float32,
    )
    rank_in = jnp.sum(jnp.where(one_hot, before, 0.0), axis=1).astype(jnp.int32)
    target = (flat_routes * capacity + rank_in).reshape(top_count, out_rows)
    slots = expert_total * capacity
    middle, outbound = pl.pallas_call(
        middle_kernel,
        out_shape=(
            jax.ShapeDtypeStruct((out_rows, model_width), jnp.bfloat16),
            jax.ShapeDtypeStruct((slots, model_width), jnp.bfloat16),
        ),
        in_specs=[VMEM] * 7,
        out_specs=(VMEM, VMEM),
        compiler_params=pltpu.CompilerParams(vmem_limit_bytes=48 * 1024 * 1024),
    )(
        whole_rows,
        out_gain[None, :],
        out_proj,
        residual,
        mid_gain[None, :],
        mid_bias[None, :],
        target,
    )
    arrived = exchange_all(
        outbound.reshape(device_total, local_experts * capacity, model_width), sp_size, tp_size, 2
    )
    grouped_rows = arrived.reshape(device_total, local_experts, capacity, model_width)
    gate_part = jnp.einsum(
        "sekd,edf->sekf", grouped_rows, expert_gate, preferred_element_type=jnp.float32
    )
    up_part = jnp.einsum(
        "sekd,edf->sekf", grouped_rows, expert_up, preferred_element_type=jnp.float32
    )
    hidden = (jax.nn.silu(gate_part) * up_part).astype(jnp.bfloat16)
    served = jnp.einsum("sekf,efd->sekd", hidden, expert_down, preferred_element_type=jnp.float32)
    returned = exchange_all(
        served.astype(jnp.bfloat16).reshape(arrived.shape), sp_size, tp_size, 3
    )
    return pl.pallas_call(
        final_kernel,
        out_shape=jax.ShapeDtypeStruct((out_rows, model_width), jnp.bfloat16),
        in_specs=[VMEM] * 6,
        out_specs=VMEM,
        compiler_params=pltpu.CompilerParams(vmem_limit_bytes=48 * 1024 * 1024),
    )(
        returned.reshape(slots, model_width),
        target.T,
        route_weights,
        middle,
        final_gain[None, :],
        final_bias[None, :],
    )


def solution(mesh):
    return jax.shard_map(
        per_device,
        mesh=mesh,
        in_specs=(
            P("sp", "tp"),
            P("sp", "tp"),
            P("sp", "tp"),
            P("sp"),
            P(),
            P(),
            P(),
            P(),
            P(("sp", "tp"), None),
            P(),
            P(),
            P(("sp", "tp"), None),
            P(("sp", "tp"), None),
            P(("sp", "tp"), None, None),
            P(("sp", "tp"), None, None),
            P(("sp", "tp"), None, None),
            P(),
            P(),
        ),
        out_specs=P(("sp", "tp"), None),
        check_vma=False,
    )
```

time: 325 us -> 202 us (0.62)
  Pallas kernels: 0 us -> 171 us
  waiting for transfers between devices: 102 us -> 0 us
  blocking collectives: 72.8 us -> 0 us
  matrix products: 62 us -> 10.9 us
  local copies, waits for them, and re-layouts: 25.6 us -> 6.79 us
  other arithmetic: 28.8 us -> 10.3 us
  between operations: 16.2 us -> 0.36 us
  starting transfers between devices: 11.2 us -> 0 us
    pallas_call x0 -> x7, Pallas kernels: none -> 171 us  [the longest x2 112 us: exchange_all(): pl.pallas_call(functools.partial(all_exchange_kernel, sp_size, tp_size),...]
    dot_general x17 -> x1, matrix products: 53.6 us -> 0.23 us  [per_device(): jnp.dot(earlier.astype(jnp.bfloat16), one_hot.astype(jnp.bfloat16), prefe...]
    all_to_all x1 -> x0, blocking collectives: 51.8 us -> none  [per_device(): lax.all_to_all(outbound.reshape(expert_total, capacity, model_width), ('s...]
    all_gather x2 -> x0, waiting for transfers between devices: 51.2 us -> none  [the longest x1 40.8 us: per_device(): value_part = lax.all_gather(value_heads, 'sp', axis=0, tiled=True)]
    all_to_all x2 -> x0, waiting for transfers between devices: 50.5 us -> none  [the longest x1 45.4 us: per_device(): lax.all_to_all(served.astype(jnp.bfloat16).reshape(arrived.shape), ('sp',...]
    all_gather x1 -> x0, blocking collectives: 21.1 us -> none  [per_device(): doc_part = lax.all_gather(documents, 'sp', axis=0, tiled=True)]
    all_to_all x2 -> x0, starting transfers between devices: 11.1 us -> none  [the longest x1 6.21 us: per_device(): lax.all_to_all(served.astype(jnp.bfloat16).reshape(arrived.shape), ('sp',...]
    add x8 -> x1, other arithmetic: 9.54 us -> 0.01 us  [per_device(): target = (flat_routes * capacity + rank_in).reshape(top_count, out_rows)]
  transfers between devices with their start and end apart: 4 -> 0, of which waited for: 4 -> 0; matrix products, arithmetic and copies ran while one was open for 1% -> 0% of each run, Pallas kernels for 0% -> 0%
where the time goes in v1:
time: 202 us; the launch traced here: 199 us
  Pallas kernels  171 us (85%)
  matrix products  10.9 us (5%)
  other arithmetic  10.3 us (5%)
  local copies, waits for them, and re-layouts  6.79 us (3%)
    pallas_call x2, Pallas kernels, exchange_all(): pl.pallas_call(functools.partial(all_exchange_kernel, sp_size, tp_size),...  112 us
    pallas_call x1, Pallas kernels, gather_keys(): pl.pallas_call(functools.partial(gather_kernel, size, pair), out_shape=(j...  32.7 us
    pallas_call x1, Pallas kernels, attend(): pl.pallas_call(functools.partial(attention_kernel, grouped), out_shape=ja...  12.2 us
    pallas_call x1, Pallas kernels, exchange_heads(): pl.pallas_call(functools.partial(head_exchange_kernel, size), out_shape=j...  8.1 us
    dot_general x1, matrix products, per_device(): jnp.einsum('sekf,efd->sekd', hidden, expert_down, preferred_element_type=...  6.23 us
    unnamed x41, local copies, waits for them, and re-layouts  5.72 us
    dot_general x1, matrix products, per_device(): jnp.einsum('sekd,edf->sekf', grouped_rows, expert_gate, preferred_element...  4.43 us

profile of v1, /device:TPU:13, one launch (start us, length us, event | category | flops | bytes accessed | tf_op | source)
XLA Modules:
  0.0 199.3 jit_solution(4328040352034184479)
XLA Ops:
  0.1 0.2 fusion.33
  0.3 0.0 copy-start.13
  0.3 1.2 fusion.24
  1.5 1.0 fusion.26
  2.5 1.2 fusion.27
  3.7 0.0 copy-start.18
  3.7 0.0 copy-done.14
  3.8 0.8 maximum_bitcast_fusion.1.kv_ref
  4.6 32.7 %shard_map.172 = (bf16[8,2,512,128]{3,2,1,0:T(8,128)(2,1)}, s32[8,4,128]{2,1,0:T(4,128)}) custom-call(bf16[2,512,128]{2,1,0:T(8,128)(2,1)} %maximum_bitcast_fusion.1.kv_ref, s32[4,128]{1,0:T(4,128)} %bitcast.99), custom_call_target="tpu_custom_call" | custom-call | tf_op jit(solution)/shard_map/pallas_call | solution.py:139
  37.3 0.6 fusion.44
  37.9 2.8 %fusion.36 = (s32[]{:T(128)}, s32[]{:T(128)}) fusion(s32[8,4,128]{2,1,0:T(4,128)} %get-tuple-element.10.doc_ref, s32[]{:T(128)} %bitcast.12, s32[]{:T(128)} %bitcast.14), kind=kLoop, calls=%fused_computation.45 | loop fusion | flops 46 | bytes 80 | tf_op jit(solution)/shard_map/reduce_sum | solution.py:392
  40.7 1.3 pad_add_fusion.range_ref
  41.9 1.1 fusion.32
  43.0 0.1 copy.31
  43.2 0.1 copy.32
  43.3 0.1 multiply_reduce_fusion
  43.4 0.2 multiply_multiply_fusion
  43.7 0.3 subtract_convert_fusion
  43.9 0.0 copy-start.16
  43.9 0.1 maximum_bitcast_fusion.q_ref
  44.1 0.0 copy-start.6
  44.1 0.0 copy-start.8
  44.1 0.0 copy-start.9
  44.1 0.0 copy-start.12
  44.2 0.1 broadcast_in_dim.15.qdoc_ref
  44.3 0.7 copy-done.2
  45.0 0.0 copy-done.7
  45.0 12.2 %shard_map.173.x_ref = bf16[512,256]{1,0:T(8,128)(2,1)S(1)} custom-call(bf16[2,512,128]{2,1,0:T(8,128)(2,1)S(1)} %maximum_bitcast_fusion.q_ref, s32[512,128]{1,0:T(8,128)S(1)} %broadcast_in_dim.15.qdoc_ref, bf16[8,2,512,128]{3,2,1,0:T(8,128)(2,1)S(1)} %copy-done.2, s32[8,4,128]{2,1,0:T(4,128)S(1)} %copy-done.7, s32[2]{0:T(128)S(1)} %pad_add_fusion.range_ref), custom_call_target="tpu_custom_call" | custom-call | tf_op jit(solution)/shard_map/pallas_call | solution.py:201
  57.2 0.0 copy-start.5
  57.2 0.7 copy-done.5
  57.9 8.1 %shard_map.174.x_ref = bf16[128,1024]{1,0:T(8,128)(2,1)} custom-call(bf16[512,256]{1,0:T(8,128)(2,1)} %copy-done.5), custom_call_target="tpu_custom_call" | custom-call | tf_op jit(solution)/shard_map/pallas_call | solution.py:240
  66.0 0.1 copy.34
  66.1 0.1 copy.36
  66.2 0.2 fusion.20
  66.4 0.1 copy.37
  66.6 0.1 copy.38.target_ref
  66.6 0.0 copy-done.9
  66.7 0.9 copy-done.4
  67.6 3.9 %shard_map.175 = (bf16[128,2048]{1,0:T(8,128)(2,1)S(1)}, bf16[512,2048]{1,0:T(8,128)(2,1)S(1)}) custom-call(bf16[128,1024]{1,0:T(8,128)(2,1)S(1)} %copy-done.4, f32[1,1024]{1,0:T(1,128)S(1)} %bitcast.95, bf16[1024,2048]{1,0:T(8,128)(2,1)} %proj_ref.1, bf16[128,2048]{1,0:T(8,128)(2,1)S(1)} %copy-done.6, f32[1,2048]{1,0:T(1,128)S(1)} %bitcast.91, ...), custom_call_target="tpu_custom_call" | custom-call | tf_op jit(solution)/shard_map/pallas_call | solution.py:426
  71.5 1.3 copy-done.3
  72.8 58.4 %shard_map.176 = bf16[32,16,2048]{2,1,0:T(8,128)(2,1)} custom-call(bf16[32,16,2048]{2,1,0:T(8,128)(2,1)} %bitcast.89), custom_call_target="tpu_custom_call" | custom-call | tf_op jit(solution)/shard_map/pallas_call | solution.py:300
  131.3 4.4 %fusion.5 = f32[32,1,16,512]{3,2,0,1:T(8,128)} fusion(bf16[32,16,2048]{2,1,0:T(8,128)(2,1)} %shard_map.176, bf16[1,2048,512]{2,1,0:T(8,128)(2,1)} %param.31), kind=kOutput, calls=%fused_computation.6 | convolution fusion | flops 1073741824 | bytes 5242880 | tf_op jit(solution)/shard_map/sekd,edf->sekf/dot_general | solution.py:448
  135.7 0.0 copy-done
  135.7 6.2 %convolution_convert_fusion.x_ref = bf16[32,16,2048]{2,1,0:T(8,128)(2,1)} fusion(bf16[1,512,2048]{2,1,0:T(8,128)(2,1)S(1)} %copy-done, bf16[32,16,2048]{2,1,0:T(8,128)(2,1)} %shard_map.176, bf16[1,2048,512]{2,1,0:T(8,128)(2,1)} %param.32, f32[32,1,16,512]{3,2,0,1:T(8,128)} %fusion.5), kind=kOutput, calls=%fused_computation | convolution fusion | flops 2150105088 | bytes 9437184 | tf_op jit(solution)/shard_map/sekf,efd->sekd/dot_general | solution.py:455
  141.9 53.7 %shard_map.177 = bf16[32,16,2048]{2,1,0:T(8,128)(2,1)} custom-call(bf16[32,16,2048]{2,1,0:T(8,128)(2,1)} %convolution_convert_fusion.x_ref), custom_call_target="tpu_custom_call" | custom-call | tf_op jit(solution)/shard_map/pallas_call | solution.py:300
  195.6 0.1 copy.39.weight_ref
  195.8 1.6 copy-done.1
  197.3 2.0 shard_map.178
  (27 shorter events, 0.1 us)
Async XLA Ops:
  0.0 135.7 %copy-start = (bf16[1,512,2048]{2,1,0:T(8,128)(2,1)S(1)}, bf16[1,512,2048]{2,1,0:T(8,128)(2,1)}, u32[]{:S(2)}) copy-start(bf16[1,512,2048]{2,1,0:T(8,128)(2,1)} %param.33) | copy-start | bytes 6291460
  0.0 3.7 %copy-start.14 = (bf16[512,128]{1,0:T(8,128)(2,1)S(1)}, bf16[512,128]{1,0:T(8,128)(2,1)}, u32[]{:S(2)}) copy-start(bf16[512,128]{1,0:T(8,128)(2,1)} %param.20) | copy-start | bytes 393220
  0.0 37.3 %copy-start.15 = (s32[512]{0:T(512)S(1)}, s32[512]{0:T(512)}, u32[]{:S(2)}) copy-start(s32[512]{0:T(512)} %param.21) | copy-start | bytes 6148
  0.3 42.8 %copy-start.13 = (bf16[512,256]{1,0:T(8,128)(2,1)S(1)}, bf16[512,256]{1,0:T(8,128)(2,1)}, u32[]{:S(2)}) copy-start(bf16[512,256]{1,0:T(8,128)(2,1)} %param.18) | copy-start | bytes 786436
  3.7 39.7 %copy-start.18 = (f32[128]{0:T(128)S(1)}, f32[128]{0:T(128)}, u32[]{:S(2)}) copy-start(f32[128]{0:T(128)} %param.22) | copy-start | bytes 1540
  43.4 1.6 copy-start.2
  43.4 1.6 copy-start.7
  43.9 22.1 %copy-start.16 = (s32[128,2]{0,1:T(2,128)S(1)}, s32[128,2]{0,1:T(2,128)}, u32[]{:S(2)}) copy-start(s32[128,2]{0,1:T(2,128)} %param.29) | copy-start | bytes 3076
  44.1 22.5 %copy-start.6 = (bf16[128,2048]{1,0:T(8,128)(2,1)S(1)}, bf16[128,2048]{1,0:T(8,128)(2,1)}, u32[]{:S(2)}) copy-start(bf16[128,2048]{1,0:T(8,128)(2,1)} %res_ref.1) | copy-start | bytes 1572868
  44.1 22.5 %copy-start.8 = (f32[2048]{0:T(1024)S(1)}, f32[2048]{0:T(1024)}, u32[]{:S(2)}) copy-start(f32[2048]{0:T(1024)} %param.27) | copy-start | bytes 24580
  44.1 22.5 %copy-start.9 = (f32[2048]{0:T(1024)S(1)}, f32[2048]{0:T(1024)}, u32[]{:S(2)}) copy-start(f32[2048]{0:T(1024)} %param.28) | copy-start | bytes 24580
  44.1 22.5 %copy-start.12 = (f32[1024]{0:T(1024)S(1)}, f32[1024]{0:T(1024)}, u32[]{:S(2)}) copy-start(f32[1024]{0:T(1024)} %param.24) | copy-start | bytes 12292
  57.2 0.7 copy-start.5
  66.7 1.0 copy-start.4
  71.5 1.3 copy-start.3
  141.9 53.7 %copy-start.17 = (f32[128,2]{0,1:T(2,128)S(1)}, f32[128,2]{0,1:T(2,128)}, u32[]{:S(2)}) copy-start(f32[128,2]{0,1:T(2,128)} %param.30) | copy-start | bytes 3076
  141.9 53.8 %copy-start.10 = (f32[2048]{0:T(1024)S(1)}, f32[2048]{0:T(1024)}, u32[]{:S(2)}) copy-start(f32[2048]{0:T(1024)} %param.34) | copy-start | bytes 24580
  141.9 53.8 %copy-start.11 = (f32[2048]{0:T(1024)S(1)}, f32[2048]{0:T(1024)}, u32[]{:S(2)}) copy-start(f32[2048]{0:T(1024)} %param.35) | copy-start | bytes 24580
  195.7 1.6 copy-start.1
